TPU v7x, 256 devices: a whole 4x4x8 slice. The times are simulated.
256 devices in a mesh: sp: 32 (over z, x), tp: 8 (over y, core).
Axes of the slice: x: 4, y: 4, z: 8, core: 2. Of those that a mesh axis runs over, the one named last changes fastest.
Arguments:
- tokens: bfloat16 [24576, 4096], P('sp', 'tp'), may hold values from -6 to 6
- norm_gain: float32 [4096], replicated, may hold values from 0.1 to 1.9
- w_query: bfloat16 [4096, 2048], P('sp', 'tp'), may hold values from -0.09375 to 0.09375
- w_key: bfloat16 [4096, 1024], P('sp', 'tp'), may hold values from -0.09375 to 0.09375
- w_value: bfloat16 [4096, 1024], P('sp', 'tp'), may hold values from -0.09375 to 0.09375
- w_pool: bfloat16 [4096, 1024], P('sp', 'tp'), may hold values from -0.09375 to 0.09375
- query_gain: float32 [64], replicated, may hold values from 0.5 to 8
- key_gain: float32 [64], replicated, may hold values from 0.5 to 8
- sink_logit: float32 [32], P('tp'), may hold values from 1 to 5
- w_out_pool: bfloat16 [1024, 4096], P('tp', 'sp'), may hold values from -0.75 to 0.75
- w_out_attn: bfloat16 [2048, 4096], P('tp', 'sp'), may hold values from -1.5 to 1.5
Outputs:
- mixed: bfloat16 [24576, 4096], P(('sp', 'tp'))
All inputs are finite; a program needn't handle non-finite values.
Results may differ from a plain program's by a relative error of at most 0.014.
The roundings to bfloat16 on the way count: a program that leaves them out, or rounds other values in their place, can miss the bound.
Values may be sent and summed in bfloat16 or wider, within the bound.
No kernel may reach another device: no remote copies, remote signals or barrier semaphores. Data moves between devices by JAX's collectives and lax.ppermute only.
A program may use at most 128 MiB of HBM per device.

v0:
```python
import jax
import jax.numpy as jnp
from jax import lax
from jax.sharding import PartitionSpec as P

HEAD = 64
POOL = 1024
WINDOW = 128
GRID_W = 64
eps = 1e-06
rope_base = 10000.0
neg_big = -1e30
pool_reach = 8


def padded_2(block, sides, width):
    for axis, dim in sides:
        count = lax.axis_size(axis)
        forward = [(i, i + 1) for i in range(count - 1)]
        backward = [(target, source) for source, target in forward]
        low = lax.ppermute(
            lax.slice_in_dim(block, block.shape[dim] - width, None, axis=dim), axis, forward
        )
        high = lax.ppermute(lax.slice_in_dim(block, 0, width, axis=dim), axis, backward)
        block = jnp.concatenate([low, block, high], axis=dim)
    return block


def sent_together(arrays, axis, dim, along):
    ends, at = ([], 0)
    for a in arrays[:-1]:
        at += a.shape[along]
        ends.append(at)
    both = jnp.concatenate(arrays, axis=along)
    return tuple(jnp.split(lax.all_gather(both, axis, axis=dim, tiled=True), ends, axis=along))


def rope_tables(positions, head_size):
    quarter = head_size // 4
    freqs = 1.0 / rope_base ** (jnp.arange(quarter, dtype=jnp.float32) * 2.0 / (head_size // 2))
    row_angle = (positions // GRID_W).astype(jnp.float32)[:, None] * freqs
    col_angle = (positions % GRID_W).astype(jnp.float32)[:, None] * freqs
    angles = jnp.concatenate([row_angle, row_angle, col_angle, col_angle], axis=-1)
    return (jnp.cos(angles), jnp.sin(angles))


def rotate(heads_in, cosine, sine):
    part_one, part_two, part_three, part_four = jnp.split(heads_in, 4, axis=-1)
    turned = jnp.concatenate([-part_two, part_one, -part_four, part_three], axis=-1)
    return heads_in * cosine[:, None, :] + turned * sine[:, None, :]


def prepare(projected, gain, cosine, sine):
    rows_count = projected.shape[0]
    shaped = projected.reshape(rows_count, -1, HEAD)
    scaled = shaped * lax.rsqrt(jnp.mean(shaped * shaped, axis=-1, keepdims=True) + eps) * gain
    return rotate(scaled, cosine, sine).reshape(rows_count, -1).astype(jnp.bfloat16)


def edge_keys(keys_new, values_new):
    joined = jnp.concatenate([keys_new, values_new], axis=1)
    return padded_2(joined, (("sp", 0),), WINDOW)


def edge_pool(pool_in):
    return padded_2(pool_in, (("sp", 0),), pool_reach)


def window_attention(queries, key_band, sink_logit, positions, seq):
    rows_count = queries.shape[0]
    key_width = key_band.shape[1] // 2
    heads_q = queries.shape[1] // HEAD
    heads_k = key_width // HEAD
    group = heads_q // heads_k
    blocks = rows_count // WINDOW
    stacked = key_band.reshape(blocks + 2, WINDOW, 2 * key_width)
    joined = jnp.concatenate([stacked[:-2], stacked[1:-1], stacked[2:]], axis=1)
    block_keys = joined[:, :, :key_width].reshape(blocks, 3 * WINDOW, heads_k, HEAD)
    block_values = joined[:, :, key_width:].reshape(blocks, 3 * WINDOW, heads_k, HEAD)
    block_queries = queries.reshape(blocks, WINDOW, heads_k, group, HEAD)
    scores = jnp.einsum(
        "nqhgd,nkhd->nhgqk", block_queries, block_keys, preferred_element_type=jnp.float32
    ) * HEAD ** (-0.5)
    query_pos = positions.reshape(blocks, WINDOW)
    key_pos = query_pos[:, :1] - WINDOW + jnp.arange(3 * WINDOW, dtype=jnp.int32)[None, :]
    inside = (
        (jnp.abs(query_pos[:, :, None] - key_pos[:, None, :]) <= WINDOW)
        & (key_pos[:, None, :] >= 0)
        & (key_pos[:, None, :] < seq)
    )
    scores = jnp.where(inside[:, None, None], scores, neg_big)
    sink = sink_logit.reshape(heads_k, group)[None, :, :, None, None]
    top = jnp.maximum(jnp.max(scores, axis=-1, keepdims=True), sink)
    raised = jnp.exp(scores - top)
    totals = jnp.sum(raised, axis=-1, keepdims=True) + jnp.exp(sink - top)
    weights = (raised / totals).astype(jnp.bfloat16)
    result = jnp.einsum(
        "nhgqk,nkhd->nqhgd", weights, block_values, preferred_element_type=jnp.float32
    )
    return result.astype(jnp.bfloat16).reshape(rows_count, heads_q * HEAD)


def window_pool(pool_band, pool_in, positions, seq):
    rows_count = pool_in.shape[0]
    level = lax.axis_index("tp") * pool_in.shape[1] // (POOL // 4)
    padded = pool_band.astype(jnp.float32)
    sum_two = padded[:-1] + padded[1:]
    sum_four = sum_two[:-2] + sum_two[2:]
    sum_eight = sum_four[:-4] + sum_four[4:]
    sum_sixteen = sum_eight[:-8] + sum_eight[8:]
    candidates = jnp.stack(
        [
            sum_two[7 : 7 + rows_count],
            sum_four[6 : 6 + rows_count],
            sum_eight[4 : 4 + rows_count],
            sum_sixteen[:rows_count],
        ]
    )
    chosen = lax.dynamic_index_in_dim(candidates, level, 0, keepdims=False)
    reach = jnp.left_shift(jnp.int32(1), level)
    low = jnp.clip(positions - reach, 0, seq - 1)
    high = jnp.clip(positions + reach - 1, 0, seq - 1)
    counted = (high - low + 1).astype(jnp.float32)
    return (chosen / counted[:, None]).astype(jnp.bfloat16)


def shards(
    tokens,
    norm_gain,
    w_query,
    w_key,
    w_value,
    w_pool,
    query_gain,
    key_gain,
    sink_logit,
    w_out_pool,
    w_out_attn,
):
    gathered = lax.all_gather(tokens, "tp", axis=1, tiled=True)
    rows_count = gathered.shape[0]
    widened = gathered.astype(jnp.float32)
    normed = (
        widened * lax.rsqrt(jnp.mean(widened * widened, axis=1, keepdims=True) + eps) * norm_gain
    ).astype(jnp.bfloat16)
    positions = lax.axis_index("sp") * rows_count + jnp.arange(rows_count, dtype=jnp.int32)
    seq = lax.axis_size("sp") * rows_count
    cosine, sine = rope_tables(positions, HEAD)
    pieces = sent_together((w_query, w_key, w_value, w_pool), "sp", 0, 1)
    query_raw, key_raw, value_raw, pool_raw = tuple(
        (jnp.dot(normed, piece, preferred_element_type=jnp.float32) for piece in pieces)
    )
    queries = prepare(query_raw, query_gain, cosine, sine)
    keys_new = prepare(key_raw, key_gain, cosine, sine)
    pool_in = pool_raw.astype(jnp.bfloat16)
    key_band = edge_keys(keys_new, value_raw.astype(jnp.bfloat16))
    pool_band = edge_pool(pool_in)
    pooled = window_pool(pool_band, pool_in, positions, seq)
    attended = window_attention(queries, key_band, sink_logit, positions, seq)
    out_pool, out_attn = sent_together((w_out_pool, w_out_attn), "sp", 1, 0)
    return lax.psum_scatter(
        (
            jnp.dot(pooled, out_pool, preferred_element_type=jnp.float32)
            + jnp.dot(attended, out_attn, preferred_element_type=jnp.float32)
        ).astype(jnp.bfloat16),
        "tp",
        scatter_dimension=0,
        tiled=True,
    )


def solution(mesh):
    placed = (
        P("sp", "tp"),
        P(),
        P("sp", "tp"),
        P("sp", "tp"),
        P("sp", "tp"),
        P("sp", "tp"),
        P(),
        P(),
        P("tp"),
        P("tp", "sp"),
        P("tp", "sp"),
    )
    return jax.shard_map(
        shards, mesh=mesh, in_specs=placed, out_specs=P(("sp", "tp"), None), check_vma=False
    )
```

profile of v0, /device:TPU:1, one launch (start us, length us, event | category | flops | bytes accessed | tf_op | source)
XLA Modules:
  0.0 294.5 jit_solution(10621798535016886993)
XLA Ops:
  6.5 0.7 all-gather.4.cloned.1.call-update
  7.3 1.6 pad_maximum_fusion.7
  9.0 1.5 pad_maximum_fusion.8
  10.9 0.7 max.27
  11.6 0.7 mul.195
  12.3 0.7 mul.217
  13.5 1.4 fusion.12
  14.9 41.9 %all-gather.4.cloned.1.call-done = bf16[768,4096]{1,0:T(8,128)(2,1)} async-done(((bf16[768,512]{1,0:T(8,128)(2,1)}), bf16[768,4096]{1,0:T(8,128)(2,1)}) %all-gather.4.cloned.1.call-update) | async-done | bytes 6291472 | tf_op jit(solution)/shard_map/all_gather | solution.py:140
  56.8 4.2 %fusion = f32[768]{0:T(1024)S(1)} fusion(bf16[768,4096]{1,0:T(8,128)(2,1)} %all-gather.4.cloned.1.call-done), kind=kLoop, calls=%fused_computation.2 | loop fusion | flops 9436416 | bytes 6294528 | tf_op jit(solution)/shard_map/reduce_sum | solution.py:144
  61.1 0.4 copy-done.1
  61.4 5.4 %fusion.2 = bf16[768,4096]{1,0:T(8,128)(2,1)} fusion(bf16[768,4096]{1,0:T(8,128)(2,1)S(1)} %copy-done.1, f32[4096]{0:T(1024)S(1)} %copy-done.3, f32[768]{0:T(1024)S(1)} %add_rsqrt_fusion.2), kind=kLoop, calls=%fused_computation.4 | loop fusion | flops 12582912 | bytes 12602368 | tf_op jit(solution)/shard_map/convert_element_type | solution.py:145
  66.8 74.1 %all-gather.6.cloned.1.call-done = bf16[4096,640]{1,0:T(8,128)(2,1)} async-done(((bf16[128,640]{1,0:T(8,128)(2,1)}), bf16[4096,640]{1,0:T(8,128)(2,1)}) %all-gather.6.cloned.1.call-update) | async-done | bytes 5242896 | tf_op jit(solution)/shard_map/all_gather | solution.py:35
  140.8 5.0 %convolution_convert_fusion.1 = bf16[768,128]{1,0:T(8,128)(2,1)S(1)} fusion(bf16[768,4096]{1,0:T(8,128)(2,1)} %fusion.2, bf16[4096,640]{1,0:T(8,128)(2,1)} %all-gather.6.cloned.1.call-done), kind=kOutput, calls=%fused_computation.26 | convolution fusion | flops 805404672 | bytes 7536640 | tf_op jit(solution)/shard_map/dot_general | solution.py:151
  145.8 1.9 collective-permute-start
  147.7 1.6 collective-permute-start.1
  149.3 3.5 %multiply_reduce_fusion.1 = (f32[768,2]{0,1:T(2,128)S(1)}, f32[768,128]{0,1:T(8,128)S(1)}) fusion(bf16[768,4096]{1,0:T(8,128)(2,1)S(1)} %copy-done, bf16[4096,640]{1,0:T(8,128)(2,1)} %all-gather.6.cloned.1.call-done), kind=kOutput, calls=%fused_computation.74 | convolution fusion | flops 805501440 | bytes 7739392 | tf_op jit(solution)/shard_map/dot_general | solution.py:151
  153.2 2.2 convolution_convert_fusion
  155.4 4.0 %collective-permute-start.2 = (bf16[128,256]{0,1:T(8,128)(2,1)S(1)}, bf16[128,256]{0,1:T(8,128)(2,1)S(1)}, u32[]{:S(2)}, u32[]{:S(2)}) collective-permute-start(bf16[128,256]{0,1:T(8,128)(2,1)S(1)} %get-tuple-element.16), channel_id=1, source_target_pairs={{0,8},{8,16},{16,24},{24,32},{32,40},{40,48},{48,56},{56,64},{64,7... | collective-permute-start | bytes 196616 | tf_op jit(solution)/shard_map/ppermute | solution.py:21
  159.4 1.5 collective-permute-start.3
  160.9 2.0 multiply_reduce_fusion
  163.4 0.5 reshape.301
  164.3 54.8 %all-gather.8.cloned.1.call-done = bf16[384,4096]{1,0:T(8,128)(2,1)} async-done(((bf16[384,128]{1,0:T(8,128)(2,1)}), bf16[384,4096]{1,0:T(8,128)(2,1)}) %all-gather.8.cloned.1.call-update) | async-done | bytes 3145744 | tf_op jit(solution)/shard_map/all_gather | solution.py:35
  219.1 7.6 %fusion.16 = f32[768,4096]{1,0:T(8,128)} fusion(bf16[384,4096]{1,0:T(8,128)(2,1)} %all-gather.8.cloned.1.call-done, s32[]{:T(128)S(6)} %select_n.33, f32[1,768,128]{2,1,0:T(8,128)S(1)} %get-tuple-element.38, f32[1,768,128]{2,1,0:T(8,128)S(1)} %get-tuple-element.39, f32[1,768,128]{2,1,0:T(8,128)S(1)} %get-tuple-element.40, ...), kind=kOutput, calls=%fused_computation.30 | convolution fusion | flops 805797888 | bytes 15207428 | tf_op jit(solution)/shard_map/dot_general | solution.py:163
  228.3 1.0 fusion.4
  229.3 1.0 fusion.3
  230.5 1.4 fusion.10
  232.1 0.5 slice-done
  232.6 1.3 slice-done.1
  233.9 1.2 slice-done.2
  235.1 0.9 copy-done.2
  236.0 4.5 %add_convert_fusion = bf16[768,4096]{1,0:T(8,128)(2,1)} fusion(f32[768,4096]{1,0:T(8,128)S(1)} %bitcast.93, bf16[384,4096]{1,0:T(8,128)(2,1)S(1)} %copy-done.2, bf16[32,8,6,128]{3,2,1,0:T(8,128)(2,1)S(1)} %bitcast.95), kind=kOutput, calls=%fused_computation.5 | convolution fusion | flops 1616904192 | bytes 21495808 | tf_op jit(solution)/shard_map/dot_general | solution.py:164
  240.6 47.4 %reduce-scatter.2.cloned.1.call-done = bf16[96,4096]{1,0:T(8,128)(2,1)} async-done(((bf16[768,4096]{1,0:T(8,128)(2,1)}), bf16[96,4096]{1,0:T(8,128)(2,1)}) %reduce-scatter.2.cloned.1.call-update) | async-done | bytes 786448 | tf_op jit(solution)/shard_map/reduce_scatter | solution.py:161
  (72 shorter events, 4.3 us)
Async XLA Ops:
  6.5 54.5 %copy-start.3 = (f32[4096]{0:T(1024)S(1)}, f32[4096]{0:T(1024)}, u32[]{:S(2)}) copy-start(f32[4096]{0:T(1024)} %param.12) | copy-start | bytes 49156
  6.5 50.3 %all-gather.4.cloned.1.call-start = ((), (), s32[]{:S(2)}) async-start(), calls=%async_computation.1 | async-start | bytes 7077888 | tf_op jit(solution)/shard_map/all_gather | solution.py:140
  7.3 133.6 %all-gather.6.cloned.1.call-start = ((), (), s32[]{:S(2)}) async-start(), calls=%async_computation.2 | async-start | bytes 5406720 | tf_op jit(solution)/shard_map/all_gather | solution.py:35
  8.9 210.1 %all-gather.8.cloned.1.call-start = ((), (), s32[]{:S(2)}) async-start(), calls=%async_computation.3 | async-start | bytes 3244032 | tf_op jit(solution)/shard_map/all_gather | solution.py:35
  10.5 277.5 %reduce-scatter.2.cloned.1.call-start = ((), (), s32[]{:S(2)}) async-start(), calls=%async_computation.4 | async-start | bytes 7077888 | tf_op jit(solution)/shard_map/reduce_scatter | solution.py:161
  56.8 4.6 %copy-start.1 = (bf16[768,4096]{1,0:T(8,128)(2,1)S(1)}, bf16[768,4096]{1,0:T(8,128)(2,1)}, u32[]{:S(2)}) copy-start(bf16[768,4096]{1,0:T(8,128)(2,1)} %all-gather.4.cloned.1.call-done) | copy-start | bytes 18874372
  140.8 8.5 %copy-start = (bf16[768,4096]{1,0:T(8,128)(2,1)S(1)}, bf16[768,4096]{1,0:T(8,128)(2,1)}, u32[]{:S(2)}) copy-start(bf16[768,4096]{1,0:T(8,128)(2,1)} %fusion.2) | copy-start | bytes 18874372
  145.8 18.1 %collective-permute-start = (bf16[8,128]{1,0:T(8,128)(2,1)S(1)}, bf16[8,128]{1,0:T(8,128)(2,1)S(1)}, u32[]{:S(2)}, u32[]{:S(2)}) collective-permute-start(bf16[8,128]{1,0:T(8,128)(2,1)S(1)} %get-tuple-element.22), channel_id=1, source_target_pairs={{0,8},{8,16},{16,24},{24,32},{32,40},{40,48},{48,56},{56,64},{64,7... | collective-permute-start | bytes 6152 | tf_op jit(solution)/shard_map/ppermute | solution.py:21
  147.7 5.4 %slice-start.3 = ((s8[5242880]{0:T(1024)(128)(4,1)}), s8[4194304]{0:T(1024)(128)(4,1)S(1)}, s32[]{:S(2)}) async-start(s8[5242880]{0:T(1024)(128)(4,1)} %bitcast.99), calls=%async_computation.8 | async-start | bytes 8388608
  147.7 5.1 %copy-start.5 = (f32[64]{0:T(128)S(1)}, f32[64]{0:T(128)}, u32[]{:S(2)}) copy-start(f32[64]{0:T(128)} %param.18) | copy-start | bytes 772
  147.7 5.4 %slice-start.4 = ((s8[5242880]{0:T(1024)(128)(4,1)}), s8[1048576]{0:T(1024)(128)(4,1)S(1)}, s32[]{:S(2)}) async-start(s8[5242880]{0:T(1024)(128)(4,1)} %bitcast.99), calls=%async_computation.9 | async-start | bytes 2097152
  147.7 16.2 %collective-permute-start.1 = (bf16[8,128]{1,0:T(8,128)(2,1)S(1)}, bf16[8,128]{1,0:T(8,128)(2,1)S(1)}, u32[]{:S(2)}, u32[]{:S(2)}) collective-permute-start(bf16[8,128]{1,0:T(8,128)(2,1)S(1)} %get-tuple-element.23), channel_id=1, source_target_pairs={{8,0},{16,8},{24,16},{32,24},{40,32},{48,40},{56,48},{64,56},{72,6... | collective-permute-start | bytes 6152 | tf_op jit(solution)/shard_map/ppermute | solution.py:24
  155.4 71.3 %collective-permute-start.2 = (bf16[128,256]{0,1:T(8,128)(2,1)S(1)}, bf16[128,256]{0,1:T(8,128)(2,1)S(1)}, u32[]{:S(2)}, u32[]{:S(2)}) collective-permute-start(bf16[128,256]{0,1:T(8,128)(2,1)S(1)} %get-tuple-element.16), channel_id=1, source_target_pairs={{0,8},{8,16},{16,24},{24,32},{32,40},{40,48},{48,56},{56,64},{64,7... | collective-permute-start | bytes 196616 | tf_op jit(solution)/shard_map/ppermute | solution.py:21
  159.4 3.5 %copy-start.4 = (f32[64]{0:T(128)S(1)}, f32[64]{0:T(128)}, u32[]{:S(2)}) copy-start(f32[64]{0:T(128)} %param.17) | copy-start | bytes 772
  159.4 67.2 %collective-permute-start.3 = (bf16[128,256]{0,1:T(8,128)(2,1)S(1)}, bf16[128,256]{0,1:T(8,128)(2,1)S(1)}, u32[]{:S(2)}, u32[]{:S(2)}) collective-permute-start(bf16[128,256]{0,1:T(8,128)(2,1)S(1)} %get-tuple-element.17), channel_id=1, source_target_pairs={{8,0},{16,8},{24,16},{32,24},{40,32},{48,40},{56,48},{64,56},{72,6... | collective-permute-start | bytes 196616 | tf_op jit(solution)/shard_map/ppermute | solution.py:24
  230.4 2.2 slice-start
  230.5 3.5 %slice-start.1 = ((s8[12582912]{0:T(1024)(128)(4,1)}), s8[4194304]{0:T(1024)(128)(4,1)S(1)}, s32[]{:S(2)}) async-start(s8[12582912]{0:T(1024)(128)(4,1)} %bitcast.92), calls=%async_computation.6 | async-start | bytes 8388608
  230.5 4.6 %slice-start.2 = ((s8[12582912]{0:T(1024)(128)(4,1)}), s8[4194304]{0:T(1024)(128)(4,1)S(1)}, s32[]{:S(2)}) async-start(s8[12582912]{0:T(1024)(128)(4,1)} %bitcast.92), calls=%async_computation.7 | async-start | bytes 8388608
  230.5 5.5 %copy-start.2 = (bf16[384,4096]{1,0:T(8,128)(2,1)S(1)}, bf16[384,4096]{1,0:T(8,128)(2,1)}, u32[]{:S(2)}) copy-start(bf16[384,4096]{1,0:T(8,128)(2,1)} %all-gather.8.cloned.1.call-done) | copy-start | bytes 9437188
Sparse Core Ops, SparseCore 0:
  9.2 47.6 all-gather.3
  59.4 81.3 all-gather.5
  143.3 75.7 all-gather.7
  240.7 47.2 reduce-scatter.1
where the time goes:
time: 295 us
  waiting for transfers between devices  219 us (74%)
  matrix products  27.1 us (9%)
  other arithmetic  17.2 us (6%)
  between operations  13.6 us (5%)
  starting transfers between devices  9 us (3%)
  local copies, waits for them, and re-layouts  8.74 us (3%)
    all_gather x2, waiting for transfers between devices, sent_together(): lax.all_gather(both, axis, axis=dim, tiled=True)  129 us
    reduce_scatter x1, waiting for transfers between devices, shards(): lax.psum_scatter((jnp.dot(pooled, out_pool, preferred_element_type=jnp.fl...  47.4 us
    all_gather x1, waiting for transfers between devices, shards(): gathered = lax.all_gather(tokens, 'tp', axis=1, tiled=True)  41.9 us
    dot_general x4, matrix products, shards(): jnp.dot(normed, piece, preferred_element_type=jnp.float32)  12.7 us
    dot_general x1, matrix products, shards(): jnp.dot(pooled, out_pool, preferred_element_type=jnp.float32)  7.6 us
  transfers between devices with their start and end apart: 8, of which 4 were waited for; matrix products, arithmetic and copies ran while one was open for 13% of the time, Pallas kernels for 0%

commit v1 on v0

--- a/solution.py
+++ b/solution.py
@@ -137,7 +137,11 @@
     w_out_pool,
     w_out_attn,
 ):
-    gathered = lax.all_gather(tokens, "tp", axis=1, tiled=True)
+    peers = lax.axis_size("tp")
+    repeats = [peers if d == 1 else 1 for d in range(tokens.ndim)]
+    gathered = lax.all_to_all(
+        jnp.tile(tokens, repeats), "tp", split_axis=1, concat_axis=1, tiled=True
+    )
     rows_count = gathered.shape[0]
     widened = gathered.astype(jnp.float32)
     normed = (

time: 295 us -> 254 us (0.86)
  waiting for transfers between devices: 219 us -> 143 us
  local copies, waits for them, and re-layouts: 8.74 us -> 26.3 us
  starting transfers between devices: 9 us -> 16.2 us
  other arithmetic: 17.2 us -> 22.3 us
  matrix products: 27.1 us -> 31.9 us
    all_gather x2, waiting for transfers between devices: 129 us -> 27.9 us  [sent_together(): lax.all_gather(both, axis, axis=dim, tiled=True)]
    all_to_all x0 -> x1, waiting for transfers between devices: none -> 67.5 us  [shards(): lax.all_to_all(jnp.tile(tokens, repeats), 'tp', split_axis=1, concat_axis...]
    all_gather x1 -> x0, waiting for transfers between devices: 41.9 us -> none  [shards(): gathered = lax.all_gather(tokens, 'tp', axis=1, tiled=True)]
    all_to_all x0 -> x1, local copies, waits for them, and re-layouts: none -> 8.66 us  [shards(): lax.all_to_all(jnp.tile(tokens, repeats), 'tp', split_axis=1, concat_axis...]
    all_to_all x0 -> x1, starting transfers between devices: none -> 7.99 us  [shards(): lax.all_to_all(jnp.tile(tokens, repeats), 'tp', split_axis=1, concat_axis...]
    dot_general x0 -> x4, local copies, waits for them, and re-layouts: none -> 5.74 us  [shards(): jnp.dot(normed, piece, preferred_element_type=jnp.float32)]
    another operation x0 -> x1, local copies, waits for them, and re-layouts: none -> 4.3 us  [shards(): jnp.tile(tokens, repeats)]
    convert_element_type x1 -> x2, other arithmetic: 5.36 us -> 8.24 us  [shards(): normed = (widened * lax.rsqrt(jnp.mean(widened * widened, axis=1, keepdim...]
  transfers between devices with their start and end apart: 8 -> 8, of which waited for: 4 -> 3; matrix products, arithmetic and copies ran while one was open for 13% -> 24% of each run, Pallas kernels for 0% -> 0%
where the time goes in v1:
time: 254 us; the launch traced here: 253 us
  waiting for transfers between devices  143 us (56%)
  matrix products  31.9 us (13%)
  local copies, waits for them, and re-layouts  26.3 us (10%)
  other arithmetic  22.3 us (9%)
  starting transfers between devices  16.2 us (6%)
  between operations  13.6 us (5%)
    all_to_all x1, waiting for transfers between devices, shards(): lax.all_to_all(jnp.tile(tokens, repeats), 'tp', split_axis=1, concat_axis...  67.5 us
    reduce_scatter x1, waiting for transfers between devices, shards(): lax.psum_scatter((jnp.dot(pooled, out_pool, preferred_element_type=jnp.fl...  47.5 us
    all_gather x2, waiting for transfers between devices, sent_together(): lax.all_gather(both, axis, axis=dim, tiled=True)  27.9 us
    dot_general x4, matrix products, shards(): jnp.dot(normed, piece, preferred_element_type=jnp.float32)  15 us
    all_to_all x1, local copies, waits for them, and re-layouts, shards(): lax.all_to_all(jnp.tile(tokens, repeats), 'tp', split_axis=1, concat_axis...  8.66 us
    convert_element_type x2, other arithmetic, shards(): normed = (widened * lax.rsqrt(jnp.mean(widened * widened, axis=1, keepdim...  8.24 us
    all_to_all x1, starting transfers between devices, shards(): lax.all_to_all(jnp.tile(tokens, repeats), 'tp', split_axis=1, concat_axis...  7.99 us
    dot_general x1, matrix products, shards(): jnp.dot(pooled, out_pool, preferred_element_type=jnp.float32)  7.59 us
  transfers between devices with their start and end apart: 8, of which 3 were waited for; matrix products, arithmetic and copies ran while one was open for 24% of the time, Pallas kernels for 0%

profile of v1, /device:TPU:1, one launch (start us, length us, event | category | flops | bytes accessed | tf_op | source)
XLA Modules:
  0.0 253.3 jit_solution(7823903011190737706)
XLA Ops:
  6.5 1.6 pad_maximum_fusion.7
  8.1 4.3 %tile.2 = bf16[768,8,512]{2,0,1:T(8,128)(2,1)} broadcast(bf16[768,512]{1,0:T(8,128)(2,1)} %param.11), dimensions={0,2} | broadcast | bytes 7077888 | tf_op jit(solution)/shard_map/tile | solution.py:143
  12.4 8.0 %all-to-all-start = ((bf16[768,8,512]{2,0,1:T(8,128)(2,1)}), bf16[768,8,512]{2,0,1:T(8,128)(2,1)}, u32[]{:S(2)}, u32[]{:S(2)}) async-start(bf16[768,8,512]{2,0,1:T(8,128)(2,1)} %tile.2), calls=%async_computation | async-start | bytes 12582912 | tf_op jit(solution)/shard_map/all_to_all | solution.py:142
  21.6 1.1 fusion.32
  22.9 1.4 fusion.9
  24.3 67.5 %all-to-all-done = bf16[768,8,512]{2,0,1:T(8,128)(2,1)} async-done(((bf16[768,8,512]{2,0,1:T(8,128)(2,1)}), bf16[768,8,512]{2,0,1:T(8,128)(2,1)}, u32[]{:S(2)}, u32[]{:S(2)}) %all-to-all-start) | async-done | bytes 6291488 | tf_op jit(solution)/shard_map/all_to_all | solution.py:142
  91.7 8.7 %copy.68 = bf16[768,8,512]{0,2,1:T(8,128)(2,1)} copy(bf16[768,8,512]{2,0,1:T(8,128)(2,1)} %all-to-all-done) | data formatting | bytes 12582912 | tf_op jit(solution)/shard_map/all_to_all | solution.py:142
  100.4 4.2 %multiply_reduce_fusion = f32[768]{0:T(1024)S(1)} fusion(bf16[768,8,512]{0,2,1:T(8,128)(2,1)} %copy.68), kind=kLoop, calls=%fused_computation.5 | loop fusion | flops 9436416 | bytes 6294528 | tf_op jit(solution)/shard_map/reduce_sum | solution.py:148
  105.0 4.1 %fusion.1 = bf16[768,4096]{0,1:T(8,128)(2,1)} fusion(bf16[768,8,512]{0,2,1:T(8,128)(2,1)S(1)} %copy-done, f32[4096]{0:T(1024)S(1)} %copy-done.7, f32[768]{0:T(1024)S(1)} %add_rsqrt_fusion.2), kind=kLoop, calls=%fused_computation.2 | loop fusion | flops 12582912 | bytes 12602368 | tf_op jit(solution)/shard_map/convert_element_type | solution.py:149
  109.1 4.1 %multiply_convert_fusion = bf16[768,8,512]{0,2,1:T(8,128)(2,1)} fusion(bf16[768,8,512]{0,2,1:T(8,128)(2,1)S(1)} %copy-done, f32[8,512]{1,0:T(8,128)S(1)} %mul.166, f32[768]{0:T(1024)S(1)} %add_rsqrt_fusion.2), kind=kLoop, calls=%fused_computation.4 | loop fusion | flops 12582912 | bytes 12602368 | tf_op jit(solution)/shard_map/convert_element_type | solution.py:149
  113.2 1.3 slice_bitcast_fusion.1
  114.5 1.3 copy.69
  115.9 4.2 %multiply_reduce_fusion.2 = (f32[768,2]{0,1:T(2,128)S(1)}, f32[768,2,64]{0,2,1:T(8,128)S(1)}) fusion(bf16[768,4096,1]{0,1,2:T(8,128)(2,1)} %bitcast.79, bf16[2,64,4096]{2,1,0:T(8,128)(2,1)} %bitcast.91), kind=kOutput, calls=%fused_computation.66 | convolution fusion | flops 805501440 | bytes 7739392 | tf_op jit(solution)/shard_map/dot_general | solution.py:155
  120.3 1.6 fusion.25
  122.0 1.1 convolution_convert_fusion
  123.1 1.4 collective-permute-start.2
  124.6 1.3 collective-permute-start.3
  126.0 3.0 %copy.76 = bf16[256,4096]{1,0:T(8,128)(2,1)} copy(bf16[256,4096]{0,1:T(8,128)(2,1)S(1)} %slice_bitcast_fusion) | data formatting | bytes 4194304 | tf_op jit(solution)/shard_map/dot_general | solution.py:155
  129.0 5.0 %convolution_convert_fusion.1 = bf16[768,128]{1,0:T(8,128)(2,1)S(1)} fusion(bf16[768,4096]{0,1:T(8,128)(2,1)} %fusion.1, bf16[4096,640]{1,0:T(8,128)(2,1)} %all-gather.3.cloned.1.call-done), kind=kOutput, calls=%fused_computation.25 | convolution fusion | flops 805404672 | bytes 7536640 | tf_op jit(solution)/shard_map/dot_general | solution.py:155
  134.0 4.0 %collective-permute-start = (bf16[8,128]{1,0:T(8,128)(2,1)S(1)}, bf16[8,128]{1,0:T(8,128)(2,1)S(1)}, u32[]{:S(2)}, u32[]{:S(2)}) collective-permute-start(bf16[8,128]{1,0:T(8,128)(2,1)S(1)} %get-tuple-element.22), channel_id=1, source_target_pairs={{0,8},{8,16},{16,24},{24,32},{32,40},{40,48},{48,56},{56,64},{64,7... | collective-permute-start | bytes 6152 | tf_op jit(solution)/shard_map/ppermute | solution.py:21
  138.0 1.5 collective-permute-start.1
  139.5 4.7 %multiply_reduce_fusion.1 = (f32[768,4]{0,1:T(4,128)S(1)}, f32[768,4,64]{0,2,1:T(8,128)S(1)}) fusion(bf16[768,4096,1]{0,1,2:T(8,128)(2,1)} %bitcast.80, bf16[4,64,4096]{2,1,0:T(8,128)(2,1)S(1)} %bitcast.84), kind=kOutput, calls=%fused_computation.35 | convolution fusion | flops 1611002880 | bytes 9187328 | tf_op jit(solution)/shard_map/dot_general | solution.py:155
  145.6 27.9 %all-gather.5.cloned.1.call-done = bf16[384,4096]{1,0:T(8,128)(2,1)} async-done(((bf16[384,128]{1,0:T(8,128)(2,1)}), bf16[384,4096]{1,0:T(8,128)(2,1)}) %all-gather.5.cloned.1.call-update) | async-done | bytes 3145744 | tf_op jit(solution)/shard_map/all_gather | solution.py:35
  173.5 7.6 %fusion.11 = f32[768,4096]{1,0:T(8,128)} fusion(bf16[384,4096]{1,0:T(8,128)(2,1)} %all-gather.5.cloned.1.call-done, s32[]{:T(128)S(6)} %select_n.33, f32[1,768,128]{2,1,0:T(8,128)S(1)} %get-tuple-element.38, f32[1,768,128]{2,1,0:T(8,128)S(1)} %get-tuple-element.39, f32[1,768,128]{2,1,0:T(8,128)S(1)} %get-tuple-element.40, ...), kind=kOutput, calls=%fused_computation.28 | convolution fusion | flops 805797888 | bytes 15207428 | tf_op jit(solution)/shard_map/dot_general | solution.py:167
  181.1 0.9 pad_maximum_fusion.4
  183.3 1.0 fusion.3
  184.3 2.0 copy-done.1
  186.3 1.1 fusion.2
  187.8 3.8 %fusion.7 = bf16[6,128,2,2,64]{1,4,3,2,0:T(8,128)(2,1)S(1)} fusion(bf16[6,384,2,64,1]{1,3,4,2,0:T(8,128)(2,1)S(1)} %bitcast.92, f32[6,2,384,128,2]{3,2,4,1,0:T(8,128)} %copy-done.1, f32[6,2,2,128]{3,2,1,0:T(2,128)S(1)} %exponential_add_fusion, f32[6,2,2,128]{3,2,1,0:T(2,128)S(1)} %broadcast_maximum_fusion, pred[6,128,384]{1,2,0:T(8,128)(4,1)S(1)} %fusion.9), kind=kOutput, calls=%fused_computation.19 | convolution fusion | flops 157089792 | bytes 6021120 | tf_op jit(solution)/shard_map/nhgqk,nkhd->nqhgd/dot_general | solution.py:97
  192.7 1.2 slice-done.2
  194.8 4.5 %add_convert_fusion = bf16[768,4096]{1,0:T(8,128)(2,1)} fusion(f32[768,4096]{1,0:T(8,128)S(1)} %bitcast.78, bf16[384,4096]{1,0:T(8,128)(2,1)S(1)} %copy-done.2, bf16[32,8,6,128]{3,2,1,0:T(8,128)(2,1)S(1)} %bitcast.87), kind=kOutput, calls=%fused_computation.3 | convolution fusion | flops 1616904192 | bytes 21495808 | tf_op jit(solution)/shard_map/dot_general | solution.py:168
  199.3 47.5 %reduce-scatter.2.cloned.1.call-done = bf16[96,4096]{1,0:T(8,128)(2,1)} async-done(((bf16[768,4096]{1,0:T(8,128)(2,1)}), bf16[96,4096]{1,0:T(8,128)(2,1)}) %reduce-scatter.2.cloned.1.call-update) | async-done | bytes 786448 | tf_op jit(solution)/shard_map/reduce_scatter | solution.py:165
  (87 shorter events, 6.9 us)
Async XLA Ops:
  6.5 106.7 %all-gather.3.cloned.1.call-start = ((), (), s32[]{:S(2)}) async-start(), calls=%async_computation.2 | async-start | bytes 5406720 | tf_op jit(solution)/shard_map/all_gather | solution.py:35
  12.4 8.0 %copy-start.8 = (bf16[256,128]{1,0:T(8,128)(2,1)S(1)}, bf16[256,128]{1,0:T(8,128)(2,1)}, u32[]{:S(2)}) copy-start(bf16[256,128]{1,0:T(8,128)(2,1)} %param.21) | copy-start | bytes 196612
  12.4 8.0 %copy-start.9 = (bf16[128,128]{1,0:T(8,128)(2,1)S(1)}, bf16[128,128]{1,0:T(8,128)(2,1)}, u32[]{:S(2)}) copy-start(bf16[128,128]{1,0:T(8,128)(2,1)} %param.20) | copy-start | bytes 98308
  12.4 8.8 %copy-start.7 = (f32[4096]{0:T(1024)S(1)}, f32[4096]{0:T(1024)}, u32[]{:S(2)}) copy-start(f32[4096]{0:T(1024)} %param.12) | copy-start | bytes 49156
  12.4 8.8 %copy-start.12 = (f32[4]{0:T(128)S(1)}, f32[4]{0:T(128)}, u32[]{:S(2)}) copy-start(f32[4]{0:T(128)} %param.19) | copy-start | bytes 52
  12.4 79.3 %all-to-all-start = ((bf16[768,8,512]{2,0,1:T(8,128)(2,1)}), bf16[768,8,512]{2,0,1:T(8,128)(2,1)}, u32[]{:S(2)}, u32[]{:S(2)}) async-start(bf16[768,8,512]{2,0,1:T(8,128)(2,1)} %tile.2), calls=%async_computation | async-start | bytes 12582912 | tf_op jit(solution)/shard_map/all_to_all | solution.py:142
  20.4 153.1 %all-gather.5.cloned.1.call-start = ((), (), s32[]{:S(2)}) async-start(), calls=%async_computation.3 | async-start | bytes 3244032 | tf_op jit(solution)/shard_map/all_gather | solution.py:35
  21.2 225.6 %reduce-scatter.2.cloned.1.call-start = ((), (), s32[]{:S(2)}) async-start(), calls=%async_computation.4 | async-start | bytes 7077888 | tf_op jit(solution)/shard_map/reduce_scatter | solution.py:165
  100.4 4.6 %copy-start = (bf16[768,8,512]{0,2,1:T(8,128)(2,1)S(1)}, bf16[768,8,512]{0,2,1:T(8,128)(2,1)}, u32[]{:S(2)}) copy-start(bf16[768,8,512]{0,2,1:T(8,128)(2,1)} %copy.68) | copy-start | bytes 18874372
  114.5 5.6 %copy-start.10 = (f32[64]{0:T(128)S(1)}, f32[64]{0:T(128)}, u32[]{:S(2)}) copy-start(f32[64]{0:T(128)} %param.18) | copy-start | bytes 772
  114.5 7.3 %slice-start.3 = ((s8[6291456]{0:T(1024)(128)(4,1)}), s8[2097152]{0:T(1024)(128)(4,1)S(1)}, s32[]{:S(2)}) async-start(s8[6291456]{0:T(1024)(128)(4,1)} %bitcast.81), calls=%async_computation.8 | async-start | bytes 4194304
  115.9 4.4 %copy-start.5 = (f32[768,64]{0,1:T(8,128)S(1)}, f32[768,64]{0,1:T(8,128)}, u32[]{:S(2)}) copy-start(f32[768,64]{0,1:T(8,128)} %get-tuple-element.24) | copy-start | bytes 589828
  115.9 6.0 %slice-start.4 = ((s8[6291456]{0:T(1024)(128)(4,1)}), s8[4194304]{0:T(1024)(128)(4,1)S(1)}, s32[]{:S(2)}) async-start(s8[6291456]{0:T(1024)(128)(4,1)} %bitcast.81), calls=%async_computation.9 | async-start | bytes 8388608
  115.9 6.1 %copy-start.4 = (bf16[4096,640]{1,0:T(8,128)(2,1)S(1)}, bf16[4096,640]{1,0:T(8,128)(2,1)}, u32[]{:S(2)}) copy-start(bf16[4096,640]{1,0:T(8,128)(2,1)} %all-gather.3.cloned.1.call-done) | copy-start | bytes 15728644
  123.1 58.0 %collective-permute-start.2 = (bf16[128,256]{0,1:T(8,128)(2,1)S(1)}, bf16[128,256]{0,1:T(8,128)(2,1)S(1)}, u32[]{:S(2)}, u32[]{:S(2)}) collective-permute-start(bf16[128,256]{0,1:T(8,128)(2,1)S(1)} %get-tuple-element.16), channel_id=1, source_target_pairs={{0,8},{8,16},{16,24},{24,32},{32,40},{40,48},{48,56},{56,64},{64,7... | collective-permute-start | bytes 196616 | tf_op jit(solution)/shard_map/ppermute | solution.py:21
  124.6 56.6 %collective-permute-start.3 = (bf16[128,256]{0,1:T(8,128)(2,1)S(1)}, bf16[128,256]{0,1:T(8,128)(2,1)}, u32[]{:S(2)}, u32[]{:S(2)}) collective-permute-start(bf16[128,256]{0,1:T(8,128)(2,1)S(1)} %get-tuple-element.17), channel_id=1, source_target_pairs={{8,0},{16,8},{24,16},{32,24},{40,32},{48,40},{56,48},{64,56},{72,6... | collective-permute-start | bytes 196616 | tf_op jit(solution)/shard_map/ppermute | solution.py:24
  129.0 10.5 %copy-start.3 = (bf16[256,4096]{1,0:T(8,128)(2,1)S(1)}, bf16[256,4096]{1,0:T(8,128)(2,1)}, u32[]{:S(2)}) copy-start(bf16[256,4096]{1,0:T(8,128)(2,1)} %copy.76) | copy-start | bytes 6291460
  134.0 11.2 %collective-permute-start = (bf16[8,128]{1,0:T(8,128)(2,1)S(1)}, bf16[8,128]{1,0:T(8,128)(2,1)S(1)}, u32[]{:S(2)}, u32[]{:S(2)}) collective-permute-start(bf16[8,128]{1,0:T(8,128)(2,1)S(1)} %get-tuple-element.22), channel_id=1, source_target_pairs={{0,8},{8,16},{16,24},{24,32},{32,40},{40,48},{48,56},{56,64},{64,7... | collective-permute-start | bytes 6152 | tf_op jit(solution)/shard_map/ppermute | solution.py:21
  138.0 7.2 %collective-permute-start.1 = (bf16[8,128]{1,0:T(8,128)(2,1)S(1)}, bf16[8,128]{1,0:T(8,128)(2,1)S(1)}, u32[]{:S(2)}, u32[]{:S(2)}) collective-permute-start(bf16[8,128]{1,0:T(8,128)(2,1)S(1)} %get-tuple-element.23), channel_id=1, source_target_pairs={{8,0},{16,8},{24,16},{32,24},{40,32},{48,40},{56,48},{64,56},{72,6... | collective-permute-start | bytes 6152 | tf_op jit(solution)/shard_map/ppermute | solution.py:24
  139.5 4.7 %copy-start.11 = (f32[64]{0:T(128)S(1)}, f32[64]{0:T(128)}, u32[]{:S(2)}) copy-start(f32[64]{0:T(128)} %param.17) | copy-start | bytes 772
  139.5 4.9 %copy-start.6 = (f32[768,64]{0,1:T(8,128)S(1)}, f32[768,64]{0,1:T(8,128)}, u32[]{:S(2)}) copy-start(f32[768,64]{0,1:T(8,128)} %get-tuple-element.25) | copy-start | bytes 589828
  184.2 2.1 copy-start.1
  187.8 4.2 %slice-start = ((s8[12582912]{0:T(1024)(128)(4,1)}), s8[4194304]{0:T(1024)(128)(4,1)S(1)}, s32[]{:S(2)}) async-start(s8[12582912]{0:T(1024)(128)(4,1)} %bitcast.77), calls=%async_computation.5 | async-start | bytes 8388608
  187.8 4.9 %slice-start.1 = ((s8[12582912]{0:T(1024)(128)(4,1)}), s8[4194304]{0:T(1024)(128)(4,1)S(1)}, s32[]{:S(2)}) async-start(s8[12582912]{0:T(1024)(128)(4,1)} %bitcast.77), calls=%async_computation.6 | async-start | bytes 8388608
  187.8 6.1 %slice-start.2 = ((s8[12582912]{0:T(1024)(128)(4,1)}), s8[4194304]{0:T(1024)(128)(4,1)S(1)}, s32[]{:S(2)}) async-start(s8[12582912]{0:T(1024)(128)(4,1)} %bitcast.77), calls=%async_computation.7 | async-start | bytes 8388608
  187.8 7.0 %copy-start.2 = (bf16[384,4096]{1,0:T(8,128)(2,1)S(1)}, bf16[384,4096]{1,0:T(8,128)(2,1)}, u32[]{:S(2)}) copy-start(bf16[384,4096]{1,0:T(8,128)(2,1)} %all-gather.5.cloned.1.call-done) | copy-start | bytes 9437188
Sparse Core Ops, SparseCore 0:
  9.9 85.4 all-gather.2
  97.8 75.6 all-gather.4
  199.4 47.3 reduce-scatter.1
